TPU v7x, 32 devices: a whole 2x2x4 slice. The times are simulated.
32 devices in a mesh: grp: 2 (over y), sp: 4 (over z), tp: 4 (over x, core).
Axes of the slice: x: 2, y: 2, z: 4, core: 2. Of those that a mesh axis runs over, the one named last changes fastest.
Arguments:
- tokens: bfloat16 [1280, 2048], P(('grp', 'sp')), parts along dimension 0, may hold values from -6 to 6
- norm_gain: float32 [2048], replicated, may hold values from 0.6 to 5
- query_weight: bfloat16 [2048, 2048], P('sp', 'tp')
- key_weight: bfloat16 [2048, 512], P('sp', 'tp')
- value_weight: bfloat16 [2048, 512], P('sp', 'tp'), may hold values from -0.125 to 0.125
- map_lambda: float32 [16], P('tp'), may hold values from 0.3 to 0.8
- head_gain: float32 [16, 128], P('tp'), may hold values from 0.1 to 1.9
- attn_out_weight: bfloat16 [2048, 2048], P('tp', 'sp'), may hold values from -0.125 to 0.125
- pool_out_weight: bfloat16 [2048, 2048], P('tp', 'sp'), may hold values from -0.09375 to 0.09375
Outputs:
- mixed_rows: bfloat16 [1280, 2048], P(('grp', 'sp', 'tp')), parts along dimension 0
- log_totals: float32 [2, 16, 1280], P(None, 'tp', ('grp', 'sp')), parts along dimension 2
There are 2 independent parts, one for each index of `grp`. A program takes and returns all parts, laid end to end along the dimension named above; an argument that names none is the same for every part. Nothing has to cross between parts.
All inputs are finite; a program needn't handle non-finite values.
Results may differ from a plain program's by a relative error of at most 0.013.
The roundings to bfloat16 on the way count: a program that leaves them out, or rounds other values in their place, can miss the bound.
Values may be sent and summed in bfloat16 or wider, within the bound.
A program may use at most 64 MiB of HBM per device.

v0:
```python
import math
import jax
import jax.numpy as jnp
from jax import lax
from jax.sharding import PartitionSpec as P

HD = 64
VD = 128
POOL_SPAN = 16
epsilon = 1e-06
very_low = -1e30


def extended(cells, sides, width):
    for axis, dim in sides:
        count = lax.axis_size(axis)
        ends = count - 1
        head = lax.slice_in_dim(cells, 0, width, axis=dim)
        tail = lax.slice_in_dim(cells, cells.shape[dim] - width, cells.shape[dim], axis=dim)
        cells = jnp.concatenate(
            [
                lax.ppermute(tail, axis, [(i, (i + 1) % count) for i in range(ends)]),
                cells,
                lax.ppermute(head, axis, [((i + 1) % count, i) for i in range(ends)]),
            ],
            axis=dim,
        )
    return cells


def add_products(totals, pieces, source):
    results = []
    for running, piece in zip(totals, pieces):
        results.append(jnp.dot(source, piece, preferred_element_type=jnp.float32))
    return tuple(results)


def on_device(
    tokens,
    norm_gain,
    query_weight,
    key_weight,
    value_weight,
    map_lambda,
    head_gain,
    attn_out_weight,
    pool_out_weight,
):
    tokens_wide = tokens.astype(jnp.float32)
    normed = (
        tokens_wide
        * lax.rsqrt(jnp.mean(tokens_wide * tokens_wide, axis=-1, keepdims=True) + epsilon)
        * norm_gain
    ).astype(jnp.bfloat16)
    row_count = normed.shape[0]
    sp_index = lax.axis_index("sp")
    tp_index = lax.axis_index("tp")
    group_width = pool_out_weight.shape[0]
    local_heads = map_lambda.shape[0]
    key_heads = value_weight.shape[1] // VD
    group_heads = local_heads // key_heads
    q_empty = jnp.zeros((row_count, query_weight.shape[1]), jnp.float32)
    k_empty = jnp.zeros((row_count, key_weight.shape[1]), jnp.float32)
    v_empty = jnp.zeros((row_count, value_weight.shape[1]), jnp.float32)
    q_acc, k_acc, v_acc = add_products(
        (q_empty, k_empty, v_empty),
        (
            lax.all_gather(query_weight, "sp", axis=0, tiled=True),
            lax.all_gather(key_weight, "sp", axis=0, tiled=True),
            lax.all_gather(value_weight, "sp", axis=0, tiled=True),
        ),
        normed,
    )
    queries = q_acc.astype(jnp.bfloat16).reshape(row_count, key_heads, group_heads, 2, HD)
    keys_flat = k_acc.astype(jnp.bfloat16)
    values_flat = v_acc.astype(jnp.bfloat16)

    def key_block(state_now, key_pair):
        maxima, totals, accums = state_now
        key_blk, val_blk = key_pair
        scores = jnp.einsum(
            "qhgmd,khmd->hgmqk", queries, key_blk, preferred_element_type=jnp.float32
        ) * HD ** (-0.5)
        highest = jnp.maximum(maxima, jnp.max(scores, axis=-1))
        factor = jnp.exp(maxima - highest)
        weights = jnp.exp(scores - highest[..., None])
        totals = totals * factor + jnp.sum(weights, axis=-1)
        accums = accums * factor[..., None] + jnp.einsum(
            "hgmqk,khe->hgmqe",
            weights.astype(jnp.bfloat16),
            val_blk,
            preferred_element_type=jnp.float32,
        )
        return ((highest, totals, accums), None)

    start_state = (
        jnp.full((key_heads, group_heads, 2, row_count), very_low, jnp.float32),
        jnp.zeros((key_heads, group_heads, 2, row_count), jnp.float32),
        jnp.zeros((key_heads, group_heads, 2, row_count, VD), jnp.float32),
    )
    key_piece = lax.all_gather(keys_flat, "sp", axis=0, tiled=True)
    val_piece = lax.all_gather(values_flat, "sp", axis=0, tiled=True)
    piece_len = key_piece.shape[0]
    block_len = math.gcd(piece_len, 512)
    key_blocks = key_piece.reshape(piece_len // block_len, block_len, key_heads, 2, HD)
    val_blocks = val_piece.reshape(piece_len // block_len, block_len, key_heads, VD)
    state_next, unused = lax.scan(key_block, start_state, (key_blocks, val_blocks))
    maxima, totals, accums = state_next
    log_parts = maxima + jnp.log(totals)
    log_totals = jnp.transpose(log_parts, (2, 0, 1, 3)).reshape(2, local_heads, row_count)
    reads = accums / totals[..., None]
    contrast = reads[:, :, 0] - map_lambda.reshape(key_heads, group_heads, 1, 1) * reads[:, :, 1]
    scaled = (
        contrast
        * lax.rsqrt(jnp.mean(contrast * contrast, axis=-1, keepdims=True) + epsilon)
        * head_gain.reshape(key_heads, group_heads, 1, VD)
    )
    attention_head_rows = (
        jnp.transpose(scaled, (2, 0, 1, 3))
        .reshape(row_count, local_heads * VD)
        .astype(jnp.bfloat16)
    )
    head_rows, log_totals = (attention_head_rows, log_totals)
    own_chan = lax.dynamic_slice_in_dim(normed, tp_index * group_width, group_width, 1)
    reach = POOL_SPAN // 2
    padded = extended(own_chan, (("sp", 0),), reach)
    window = jnp.left_shift(jnp.int32(2), tp_index)
    half_span = window // 2
    running = jnp.zeros((row_count, group_width), jnp.float32)
    for offset in range(POOL_SPAN):
        piece = lax.dynamic_slice_in_dim(padded, reach - half_span + offset, row_count, 0).astype(
            jnp.float32
        )
        running = running + jnp.where(offset < window, piece, 0.0)
    seq_len = row_count * lax.axis_size("sp")
    position = sp_index * row_count + jnp.arange(row_count, dtype=jnp.int32)
    lower_edge = jnp.clip(position - half_span, 0, seq_len)
    upper_edge = jnp.clip(position + window - half_span, 0, seq_len)
    counts_f = (upper_edge - lower_edge).astype(jnp.float32)[:, None]
    pooled = (running / counts_f - own_chan.astype(jnp.float32)).astype(jnp.bfloat16)
    attn_whole, pool_whole = (
        lax.all_gather(attn_out_weight, "sp", axis=1, tiled=True),
        lax.all_gather(pool_out_weight, "sp", axis=1, tiled=True),
    )
    mixed = lax.psum_scatter(
        (
            jnp.dot(head_rows, attn_whole, preferred_element_type=jnp.float32)
            + jnp.dot(pooled, pool_whole, preferred_element_type=jnp.float32)
        ).astype(jnp.bfloat16),
        "tp",
        scatter_dimension=0,
        tiled=True,
    )
    return (mixed, log_totals)


def solution(mesh):
    placed = (
        P(("grp", "sp"), None),
        P(),
        P("sp", "tp"),
        P("sp", "tp"),
        P("sp", "tp"),
        P("tp"),
        P("tp", None),
        P("tp", "sp"),
        P("tp", "sp"),
    )
    return jax.shard_map(
        on_device,
        mesh=mesh,
        in_specs=placed,
        out_specs=(P(("grp", "sp", "tp"), None), P(None, "tp", ("grp", "sp"))),
        check_vma=False,
    )
```

profile of v0, /device:TPU:0, one launch (start us, length us, event | category | flops | bytes accessed | tf_op | source)
XLA Modules:
  0.0 200.9 jit_solution(6198464641306412881)
XLA Ops:
  7.2 0.0 all-gather.4.cloned.1.call-start
  7.2 0.7 all-gather.4.cloned.1.call-update
  7.9 0.0 all-gather.6.cloned.1.call-start
  8.0 0.7 all-gather.6.cloned.1.call-update
  8.7 0.0 all-gather.8.cloned.1.call-start
  8.7 1.3 fusion.15
  10.0 1.0 fusion.17
  11.0 5.0 %collective-permute-start = (bf16[8,512]{1,0:T(8,128)(2,1)S(1)}, bf16[8,512]{1,0:T(8,128)(2,1)S(1)}, u32[]{:S(2)}, u32[]{:S(2)}) collective-permute-start(bf16[8,512]{1,0:T(8,128)(2,1)S(1)} %get-tuple-element.102), channel_id=1, source_target_pairs={{0,4},{4,8},{8,12},{1,5},{5,9},{9,13},{2,6},{6,10},{10,14},{3,7},{... | collective-permute-start | bytes 24584 | tf_op jit(solution)/shard_map/ppermute | solution.py:22
  16.0 1.3 collective-permute-start.1
  17.3 0.0 all-gather.8.cloned.1.call-update
  17.3 0.0 reduce-scatter.2.cloned.1.call-start
  17.4 24.1 %all_gather.21 = bf16[2048,128]{1,0:T(8,128)(2,1)S(1)} all-gather(bf16[512,128]{1,0:T(8,128)(2,1)S(1)} %copy-done.1), channel_id=1, replica_groups=mesh['grp'=2,'sp'=4,'tp'=4] {'sp'}, dimensions={0}, use_global_device_ids=true | all-gather | bytes 655360 | tf_op jit(solution)/shard_map/all_gather | solution.py:69
  41.5 0.3 convolution_convert_fusion.2
  41.9 15.2 %all_gather.22 = bf16[640,128]{1,0:T(8,128)(2,1)S(1)} all-gather(bf16[160,128]{1,0:T(8,128)(2,1)S(1)} %convolution_convert_fusion.2), channel_id=1, replica_groups=mesh['grp'=2,'sp'=4,'tp'=4] {'sp'}, dimensions={0}, use_global_device_ids=true | all-gather | bytes 204800 | tf_op jit(solution)/shard_map/all_gather | solution.py:101
  57.1 21.5 %all_gather.24 = bf16[2048,128]{1,0:T(8,128)(2,1)S(1)} all-gather(bf16[512,128]{1,0:T(8,128)(2,1)S(1)} %copy-done.2), channel_id=1, replica_groups=mesh['grp'=2,'sp'=4,'tp'=4] {'sp'}, dimensions={0}, use_global_device_ids=true | all-gather | bytes 655360 | tf_op jit(solution)/shard_map/all_gather | solution.py:70
  78.5 0.3 convolution_convert_fusion.1
  78.9 14.8 %all_gather.25 = bf16[640,128]{1,0:T(8,128)(2,1)S(1)} all-gather(bf16[160,128]{1,0:T(8,128)(2,1)S(1)} %convolution_convert_fusion.1), channel_id=1, replica_groups=mesh['grp'=2,'sp'=4,'tp'=4] {'sp'}, dimensions={0}, use_global_device_ids=true | all-gather | bytes 204800 | tf_op jit(solution)/shard_map/all_gather | solution.py:102
  93.7 0.2 reshape.142
  93.8 0.2 copy.22
  94.2 0.0 all-gather.4.cloned.1.call-done
  94.2 2.1 %convolution_convert_fusion = bf16[160,512]{1,0:T(8,128)(2,1)S(1)} fusion(bf16[160,2048]{1,0:T(8,128)(2,1)S(1)} %fusion.17, bf16[2048,512]{1,0:T(8,128)(2,1)} %all-gather.4.cloned.1.call-done), kind=kOutput, calls=%fused_computation.29 | convolution fusion | flops 335626240 | bytes 2916352 | tf_op jit(solution)/shard_map/dot_general | solution.py:34
  96.4 0.1 copy.21
  96.6 8.5 %while.15 = (s32[]{:T(128)}, f32[1,4,2,160]{3,1,2,0:T(4,128)S(1)}, f32[1,4,2,160]{3,1,2,0:T(4,128)S(1)}, f32[1,4,2,160,128]{4,3,2,1,0:T(8,128)S(1)}, bf16[5,128,...) while((s32[]{:T(128)}, f32[1,4,2,160]{3,1,2,0:T(4,128)S(1)}, ...), condition=%wide.region_4.5_spmd.clone, body=%wide.region_1.4_spmd.clone.sunk | while | flops 64232960 | bytes 3694705 | solution.py:107
  96.6 0.6 fusion.78
  97.2 0.6 fusion.80
  97.8 0.4 fusion.81
  98.3 0.6 fusion.78
  98.9 0.6 fusion.80
  99.5 0.4 fusion.81
  100.0 0.6 fusion.78
  100.6 0.6 fusion.80
  101.2 0.4 fusion.81
  101.7 0.6 fusion.78
  102.3 0.6 fusion.80
  102.9 0.4 fusion.81
  103.4 0.6 fusion.78
  104.0 0.6 fusion.80
  104.6 0.4 fusion.81
  105.1 0.2 broadcast_divide_fusion
  105.3 0.3 multiply_reduce_fusion
  105.6 0.2 fusion.20
  105.8 0.1 copy.27
  105.9 16.4 %all-gather.6.cloned.1.call-done = bf16[512,2048]{1,0:T(8,128)(2,1)} async-done(((bf16[512,512]{1,0:T(8,128)(2,1)}), bf16[512,2048]{1,0:T(8,128)(2,1)}) %all-gather.6.cloned.1.call-update) | async-done | bytes 2097168 | tf_op jit(solution)/shard_map/all_gather | solution.py:142
  122.4 2.1 %fusion.21 = f32[160,2048]{1,0:T(8,128)S(1)} fusion(bf16[512,2048]{1,0:T(8,128)(2,1)} %all-gather.6.cloned.1.call-done, bf16[20,8,4,128]{3,2,1,0:T(4,128)(2,1)S(1)} %bitcast.102), kind=kOutput, calls=%fused_computation.42 | convolution fusion | flops 335544320 | bytes 3571712 | tf_op jit(solution)/shard_map/dot_general | solution.py:147
  124.5 44.1 %all-gather.8.cloned.1.call-done = bf16[512,2048]{1,0:T(8,128)(2,1)} async-done(((bf16[512,512]{1,0:T(8,128)(2,1)}), bf16[512,2048]{1,0:T(8,128)(2,1)}) %all-gather.8.cloned.1.call-update) | async-done | bytes 2097168 | tf_op jit(solution)/shard_map/all_gather | solution.py:143
  168.6 4.3 %fusion.14 = bf16[160,2048]{1,0:T(8,128)(2,1)} fusion(f32[160,2048]{1,0:T(8,128)S(1)} %fusion.21, bf16[512,2048]{1,0:T(8,128)(2,1)} %all-gather.8.cloned.1.call-done, bf16[160,512]{1,0:T(8,128)(2,1)S(1)} %constant_dynamic-slice_fusion.1, f32[160]{0:T(256)S(1)} %subtract_convert_fusion.2, bf16[176,512]{1,0:T(8,128)(2,1)S(1)} %pad_maximum_fusion, ...), kind=kOutput, calls=%fused_computation.23 | convolution fusion | flops 340377600 | bytes 6849616 | tf_op jit(solution)/shard_map/dot_general | solution.py:148
  172.9 0.6 add_bitcast_fusion
  173.5 20.8 %reduce-scatter.2.cloned.1.call-done = bf16[40,2048]{1,0:T(8,128)(2,1)} async-done(((bf16[160,2048]{1,0:T(8,128)(2,1)}), bf16[40,2048]{1,0:T(8,128)(2,1)}) %reduce-scatter.2.cloned.1.call-update) | async-done | bytes 163856 | tf_op jit(solution)/shard_map/reduce_scatter | solution.py:145
  (44 shorter events, 0.4 us)
Async XLA Ops:
  7.2 2.9 %copy-start = (bf16[160,2048]{1,0:T(8,128)(2,1)S(1)}, bf16[160,2048]{1,0:T(8,128)(2,1)}, u32[]{:S(2)}) copy-start(bf16[160,2048]{1,0:T(8,128)(2,1)} %param.11) | copy-start | bytes 1966084
  7.2 10.3 %copy-start.1 = (bf16[512,128]{1,0:T(8,128)(2,1)S(1)}, bf16[512,128]{1,0:T(8,128)(2,1)}, u32[]{:S(2)}) copy-start(bf16[512,128]{1,0:T(8,128)(2,1)} %param.14) | copy-start | bytes 393220
  7.2 87.0 %all-gather.4.cloned.1.call-start = ((), (), s32[]{:S(2)}) async-start(), calls=%async_computation.1 | async-start | bytes 2621440 | tf_op jit(solution)/shard_map/all_gather | solution.py:68
  7.9 114.4 %all-gather.6.cloned.1.call-start = ((), (), s32[]{:S(2)}) async-start(), calls=%async_computation.2 | async-start | bytes 2621440 | tf_op jit(solution)/shard_map/all_gather | solution.py:142
  8.7 159.9 %all-gather.8.cloned.1.call-start = ((), (), s32[]{:S(2)}) async-start(), calls=%async_computation.3 | async-start | bytes 2621440 | tf_op jit(solution)/shard_map/all_gather | solution.py:143
  10.0 47.0 %copy-start.2 = (bf16[512,128]{1,0:T(8,128)(2,1)S(1)}, bf16[512,128]{1,0:T(8,128)(2,1)}, u32[]{:S(2)}) copy-start(bf16[512,128]{1,0:T(8,128)(2,1)} %param.15) | copy-start | bytes 393220
  11.0 83.1 %collective-permute-start = (bf16[8,512]{1,0:T(8,128)(2,1)S(1)}, bf16[8,512]{1,0:T(8,128)(2,1)S(1)}, u32[]{:S(2)}, u32[]{:S(2)}) collective-permute-start(bf16[8,512]{1,0:T(8,128)(2,1)S(1)} %get-tuple-element.102), channel_id=1, source_target_pairs={{0,4},{4,8},{8,12},{1,5},{5,9},{9,13},{2,6},{6,10},{10,14},{3,7},{... | collective-permute-start | bytes 24584 | tf_op jit(solution)/shard_map/ppermute | solution.py:22
  16.0 78.2 %collective-permute-start.1 = (bf16[8,512]{1,0:T(8,128)(2,1)S(1)}, bf16[8,512]{1,0:T(8,128)(2,1)S(1)}, u32[]{:S(2)}, u32[]{:S(2)}) collective-permute-start(bf16[8,512]{1,0:T(8,128)(2,1)S(1)} %get-tuple-element.103), channel_id=1, source_target_pairs={{4,0},{8,4},{12,8},{5,1},{9,5},{13,9},{6,2},{10,6},{14,10},{7,3},{... | collective-permute-start | bytes 24584 | tf_op jit(solution)/shard_map/ppermute | solution.py:24
  17.3 177.0 %reduce-scatter.2.cloned.1.call-start = ((), (), s32[]{:S(2)}) async-start(), calls=%async_computation.4 | async-start | bytes 819200 | tf_op jit(solution)/shard_map/reduce_scatter | solution.py:145
  96.5 8.8 %copy-start.4 = (f32[4]{0:T(128)S(1)}, f32[4]{0:T(128)}, u32[]{:S(2)}) copy-start(f32[4]{0:T(128)} %param.16) | copy-start | bytes 52
  96.5 9.1 %copy-start.3 = (f32[4,128]{1,0:T(4,128)S(1)}, f32[4,128]{1,0:T(4,128)}, u32[]{:S(2)}) copy-start(f32[4,128]{1,0:T(4,128)} %param.17) | copy-start | bytes 6148
Sparse Core Ops, SparseCore 0:
  9.6 66.0 all-gather.3
  77.3 45.0 all-gather.5
  123.9 44.6 all-gather.7
  173.1 21.2 reduce-scatter.1
where the time goes:
time: 201 us
  waiting for transfers between devices  82.8 us (41%)
  blocking collectives  75.5 us (38%)
  matrix products  14.4 us (7%)
  between operations  14.2 us (7%)
  other arithmetic  6.68 us (3%)
  starting transfers between devices  6.4 us (3%)
    all_gather x1, waiting for transfers between devices, on_device(): lax.all_gather(pool_out_weight, 'sp', axis=1, tiled=True)  44.1 us
    all_gather x1, blocking collectives, on_device(): lax.all_gather(key_weight, 'sp', axis=0, tiled=True)  24.1 us
    all_gather x1, blocking collectives, on_device(): lax.all_gather(value_weight, 'sp', axis=0, tiled=True)  21.5 us
    reduce_scatter x1, waiting for transfers between devices, on_device(): lax.psum_scatter((jnp.dot(head_rows, attn_whole, preferred_element_type=j...  20.8 us
    all_gather x1, waiting for transfers between devices, on_device(): lax.all_gather(attn_out_weight, 'sp', axis=1, tiled=True)  16.4 us
    all_gather x1, blocking collectives, on_device(): key_piece = lax.all_gather(keys_flat, 'sp', axis=0, tiled=True)  15.2 us
    all_gather x1, blocking collectives, on_device(): val_piece = lax.all_gather(values_flat, 'sp', axis=0, tiled=True)  14.8 us
    ppermute x1, starting transfers between devices, extended(): lax.ppermute(tail, axis, [(i, (i + 1) % count) for i in range(ends)])  4.96 us
  transfers between devices with their start and end apart: 6, of which 3 were waited for; matrix products, arithmetic and copies ran while one was open for 9% of the time, Pallas kernels for 0%

commit v1 on v0

--- a/solution.py
+++ b/solution.py
@@ -46,6 +46,27 @@
     attn_out_weight,
     pool_out_weight,
 ):
+
+    def meet_loads(mine_x, link_axis, axis_no):
+        parts_seen = []
+        n_lanes = lax.axis_size(link_axis)
+        for rr in [*range(n_lanes)]:
+            parts_seen.append((rr, (rr + 1) % n_lanes))
+        sheets = []
+        for rr in tuple(range(n_lanes)):
+            sheets.append((rr, (rr - 1) % n_lanes))
+        arr_now, h_now = ([mine_x], [mine_x])
+        for _ in range(n_lanes // 2):
+            arr_now.append(lax.ppermute(arr_now[-1], axis_name=link_axis, perm=parts_seen))
+        for _ in tuple(range((n_lanes - 1) // 2)):
+            h_now.append(lax.ppermute(h_now[-1], axis_name=link_axis, perm=sheets))
+        before = jnp.concatenate([*arr_now[::-1], *h_now[1:]], axis=axis_no)
+        return jnp.roll(
+            before,
+            shift=(lax.axis_index(link_axis) - n_lanes // 2) * mine_x.shape[axis_no],
+            axis=axis_no,
+        )
+
     tokens_wide = tokens.astype(jnp.float32)
     normed = (
         tokens_wide
@@ -140,7 +161,7 @@
     pooled = (running / counts_f - own_chan.astype(jnp.float32)).astype(jnp.bfloat16)
     attn_whole, pool_whole = (
         lax.all_gather(attn_out_weight, "sp", axis=1, tiled=True),
-        lax.all_gather(pool_out_weight, "sp", axis=1, tiled=True),
+        meet_loads(pool_out_weight, "sp", 1),
     )
     mixed = lax.psum_scatter(
         (

time: 201 us -> 226 us (1.12)
  blocking collectives: 75.5 us -> 136 us
  waiting for transfers between devices: 82.8 us -> 24.2 us
  local copies, waits for them, and re-layouts: 0.68 us -> 11.7 us
  matrix products: 14.4 us -> 21.7 us
  starting transfers between devices: 6.4 us -> 9.04 us
    all_gather x1 -> x0, waiting for transfers between devices: 44.1 us -> none  [on_device(): lax.all_gather(pool_out_weight, 'sp', axis=1, tiled=True)]
    all_gather x1, blocking collectives: 24.1 us -> 58 us  [on_device(): lax.all_gather(key_weight, 'sp', axis=0, tiled=True)]
    all_gather x1, blocking collectives: 15.2 us -> 45.6 us  [on_device(): key_piece = lax.all_gather(keys_flat, 'sp', axis=0, tiled=True)]
    all_gather x1, waiting for transfers between devices: 16.4 us -> 0.02 us  [on_device(): lax.all_gather(attn_out_weight, 'sp', axis=1, tiled=True)]
    unnamed x12 -> x21, local copies, waits for them, and re-layouts: 0.23 us -> 8.13 us
    ppermute x0 -> x3, starting transfers between devices: none -> 5.8 us  [the longest x2 3.7 us: meet_loads(): lax.ppermute(arr_now[-1], axis_name=link_axis, perm=parts_seen)]
    dot_general x5, matrix products: 3.18 us -> 6.96 us  [key_block(): jnp.einsum('qhgmd,khmd->hgmqk', queries, key_blk, preferred_element_type=...]
    dot_general x5, matrix products: 1.94 us -> 5.61 us  [key_block(): jnp.einsum('hgmqk,khe->hgmqe', weights.astype(jnp.bfloat16), val_blk, pre...]
  transfers between devices with their start and end apart: 6 -> 8, of which waited for: 3 -> 1; matrix products, arithmetic and copies ran while one was open for 9% -> 16% of each run, Pallas kernels for 0% -> 0%
where the time goes in v1:
time: 226 us; the launch traced here: 225 us
  blocking collectives  136 us (60%)
  waiting for transfers between devices  24.2 us (11%)
  matrix products  21.7 us (10%)
  between operations  14 us (6%)
  local copies, waits for them, and re-layouts  11.7 us (5%)
  starting transfers between devices  9.04 us (4%)
  other arithmetic  8.66 us (4%)
    all_gather x1, blocking collectives, on_device(): lax.all_gather(key_weight, 'sp', axis=0, tiled=True)  58 us
    all_gather x1, blocking collectives, on_device(): key_piece = lax.all_gather(keys_flat, 'sp', axis=0, tiled=True)  45.6 us
    reduce_scatter x1, waiting for transfers between devices, on_device(): lax.psum_scatter((jnp.dot(head_rows, attn_whole, preferred_element_type=j...  23.4 us
    all_gather x1, blocking collectives, on_device(): lax.all_gather(value_weight, 'sp', axis=0, tiled=True)  18 us
    all_gather x1, blocking collectives, on_device(): val_piece = lax.all_gather(values_flat, 'sp', axis=0, tiled=True)  14.2 us
    unnamed x21, local copies, waits for them, and re-layouts  8.13 us
    dot_general x5, matrix products, key_block(): jnp.einsum('qhgmd,khmd->hgmqk', queries, key_blk, preferred_element_type=...  6.96 us
    dot_general x5, matrix products, key_block(): jnp.einsum('hgmqk,khe->hgmqe', weights.astype(jnp.bfloat16), val_blk, pre...  5.61 us
  transfers between devices with their start and end apart: 8, of which 1 were waited for; matrix products, arithmetic and copies ran while one was open for 16% of the time, Pallas kernels for 0%

profile of v1, /device:TPU:0, one launch (start us, length us, event | category | flops | bytes accessed | tf_op | source)
XLA Modules:
  0.0 225.3 jit_solution(9163375397561729329)
XLA Ops:
  7.2 0.7 all-gather.3.cloned.1.call-update
  8.0 3.1 %collective-permute-start.2 = (bf16[512,512]{1,0:T(8,128)(2,1)}, bf16[512,512]{1,0:T(8,128)(2,1)S(1)}, u32[]{:S(2)}, u32[]{:S(2)}) collective-permute-start(bf16[512,512]{1,0:T(8,128)(2,1)} %param.19), channel_id=1, source_target_pairs={{0,4},{4,8},{8,12},{12,0},{1,5},{5,9},{9,13},{13,1},{2,6},{6,10},{... | collective-permute-start | bytes 1572872 | tf_op jit(solution)/shard_map/ppermute | solution.py:60
  11.1 2.1 collective-permute-start.4
  13.2 1.3 fusion.16
  14.5 1.3 fusion.18
  15.8 1.8 collective-permute-start
  17.6 1.3 collective-permute-start.1
  19.1 58.0 %all_gather.18 = bf16[2048,128]{1,0:T(8,128)(2,1)S(1)} all-gather(bf16[512,128]{1,0:T(8,128)(2,1)} %param.14), channel_id=1, replica_groups=mesh['grp'=2,'sp'=4,'tp'=4] {'sp'}, dimensions={0}, use_global_device_ids=true | all-gather | bytes 655360 | tf_op jit(solution)/shard_map/all_gather | solution.py:90
  77.1 0.7 constant_dynamic-slice_fusion.1
  77.7 18.0 %all_gather.21 = bf16[2048,128]{1,0:T(8,128)(2,1)S(1)} all-gather(bf16[512,128]{1,0:T(8,128)(2,1)S(1)} %copy-done.3), channel_id=1, replica_groups=mesh['grp'=2,'sp'=4,'tp'=4] {'sp'}, dimensions={0}, use_global_device_ids=true | all-gather | bytes 655360 | tf_op jit(solution)/shard_map/all_gather | solution.py:91
  95.7 0.3 convolution_convert_fusion.2
  96.0 0.6 collective-permute-start.3
  96.7 45.6 %all_gather.19 = bf16[640,128]{1,0:T(8,128)(2,1)} all-gather(bf16[160,128]{1,0:T(8,128)(2,1)S(1)} %convolution_convert_fusion.2), channel_id=1, replica_groups=mesh['grp'=2,'sp'=4,'tp'=4] {'sp'}, dimensions={0}, use_global_device_ids=true | all-gather | bytes 204800 | tf_op jit(solution)/shard_map/all_gather | solution.py:122
  142.2 0.3 convolution_convert_fusion.1
  142.6 14.2 %all_gather.22 = bf16[640,128]{1,0:T(8,128)(2,1)} all-gather(bf16[160,128]{1,0:T(8,128)(2,1)S(1)} %convolution_convert_fusion.1), channel_id=1, replica_groups=mesh['grp'=2,'sp'=4,'tp'=4] {'sp'}, dimensions={0}, use_global_device_ids=true | all-gather | bytes 204800 | tf_op jit(solution)/shard_map/all_gather | solution.py:123
  156.7 1.8 reshape.142
  158.6 1.8 copy.22
  160.4 1.6 pad_maximum_fusion
  162.0 0.9 constant_dynamic-update-slice_fusion.7
  162.9 0.9 constant_dynamic-update-slice_fusion.6
  163.7 0.9 constant_dynamic-update-slice_fusion.5
  164.6 0.9 constant_dynamic-update-slice_fusion.4
  165.5 0.9 constant_dynamic-update-slice_fusion.3
  166.4 0.9 constant_dynamic-update-slice_fusion.2
  167.4 0.9 constant_dynamic-update-slice_fusion.1
  168.3 0.9 constant_dynamic-update-slice_fusion
  169.1 2.1 convolution_convert_fusion
  171.4 16.0 %while.15 = (s32[]{:T(128)}, f32[1,4,2,160]{3,1,2,0:T(4,128)S(1)}, f32[1,4,2,160]{3,1,2,0:T(4,128)S(1)}, f32[1,4,2,160,128]{4,3,2,1,0:T(8,128)S(1)}, bf16[5,128,...) while((s32[]{:T(128)}, f32[1,4,2,160]{3,1,2,0:T(4,128)S(1)}, ...), condition=%wide.region_4.5_spmd.clone, body=%wide.region_1.4_spmd.clone.sunk | while | flops 64232960 | bytes 3593337 | solution.py:128
  171.5 1.4 fusion.78
  172.9 0.6 fusion.80
  173.5 1.1 fusion.81
  174.6 1.4 fusion.78
  176.1 0.6 fusion.80
  176.7 1.1 fusion.81
  177.8 1.4 fusion.78
  179.3 0.6 fusion.80
  179.9 1.1 fusion.81
  181.0 1.4 fusion.78
  182.5 0.6 fusion.80
  183.1 1.1 fusion.81
  184.2 1.4 fusion.78
  185.7 0.6 fusion.80
  186.3 1.1 fusion.81
  187.7 0.3 multiply_reduce_fusion
  188.3 2.1 fusion.22
  190.4 4.3 %fusion.14 = bf16[160,2048]{1,0:T(8,128)(2,1)} fusion(f32[160,2048]{1,0:T(8,128)S(1)} %fusion.22, bf16[512,4096]{1,0:T(8,128)(2,1)} %constant_dynamic-update-slice_fusion, s32[]{:T(128)S(6)} %select_n.217, bf16[160,512]{1,0:T(8,128)(2,1)S(1)} %copy-done.1, f32[160]{0:T(256)S(1)} %subtract_convert_fusion.2, bf16[176,512]{1,0:T(8,128)(2,1)S(1)} %copy-done.2, ...), kind=kOutput, calls=%fused_computation.23 | convolution fusion | flops 340377600 | bytes 6849620 | tf_op jit(solution)/shard_map/dot_general | solution.py:169
  194.7 0.6 add_bitcast_fusion
  195.4 23.4 %reduce-scatter.2.cloned.1.call-done = bf16[40,2048]{1,0:T(8,128)(2,1)} async-done(((bf16[160,2048]{1,0:T(8,128)(2,1)}), bf16[40,2048]{1,0:T(8,128)(2,1)}) %reduce-scatter.2.cloned.1.call-update) | async-done | bytes 163856 | tf_op jit(solution)/shard_map/reduce_scatter | solution.py:166
  (57 shorter events, 1.1 us)
Async XLA Ops:
  7.2 70.6 %copy-start.3 = (bf16[512,128]{1,0:T(8,128)(2,1)S(1)}, bf16[512,128]{1,0:T(8,128)(2,1)}, u32[]{:S(2)}) copy-start(bf16[512,128]{1,0:T(8,128)(2,1)} %param.15) | copy-start | bytes 393220
  7.2 162.0 %all-gather.3.cloned.1.call-start = ((), (), s32[]{:S(2)}) async-start(), calls=%async_computation.1 | async-start | bytes 2621440 | tf_op jit(solution)/shard_map/all_gather | solution.py:89
  7.9 180.4 %all-gather.5.cloned.1.call-start = ((), (), s32[]{:S(2)}) async-start(), calls=%async_computation.2 | async-start | bytes 2621440 | tf_op jit(solution)/shard_map/all_gather | solution.py:163
  8.0 88.1 %collective-permute-start.2 = (bf16[512,512]{1,0:T(8,128)(2,1)}, bf16[512,512]{1,0:T(8,128)(2,1)S(1)}, u32[]{:S(2)}, u32[]{:S(2)}) collective-permute-start(bf16[512,512]{1,0:T(8,128)(2,1)} %param.19), channel_id=1, source_target_pairs={{0,4},{4,8},{8,12},{12,0},{1,5},{5,9},{9,13},{13,1},{2,6},{6,10},{... | collective-permute-start | bytes 1572872 | tf_op jit(solution)/shard_map/ppermute | solution.py:60
  11.1 153.6 %collective-permute-start.4 = (bf16[512,512]{1,0:T(8,128)(2,1)}, bf16[512,512]{1,0:T(8,128)(2,1)S(1)}, u32[]{:S(2)}, u32[]{:S(2)}) collective-permute-start(bf16[512,512]{1,0:T(8,128)(2,1)} %param.19), channel_id=1, source_target_pairs={{0,12},{4,0},{8,4},{12,8},{1,13},{5,1},{9,5},{13,9},{2,14},{6,2},{... | collective-permute-start | bytes 1572872 | tf_op jit(solution)/shard_map/ppermute | solution.py:62
  15.8 144.6 %collective-permute-start = (bf16[8,512]{1,0:T(8,128)(2,1)S(1)}, bf16[8,512]{1,0:T(8,128)(2,1)S(1)}, u32[]{:S(2)}, u32[]{:S(2)}) collective-permute-start(bf16[8,512]{1,0:T(8,128)(2,1)S(1)} %get-tuple-element.102), channel_id=1, source_target_pairs={{0,4},{4,8},{8,12},{1,5},{5,9},{9,13},{2,6},{6,10},{10,14},{3,7},{... | collective-permute-start | bytes 24584 | tf_op jit(solution)/shard_map/ppermute | solution.py:22
  17.6 142.7 %collective-permute-start.1 = (bf16[8,512]{1,0:T(8,128)(2,1)S(1)}, bf16[8,512]{1,0:T(8,128)(2,1)S(1)}, u32[]{:S(2)}, u32[]{:S(2)}) collective-permute-start(bf16[8,512]{1,0:T(8,128)(2,1)S(1)} %get-tuple-element.103), channel_id=1, source_target_pairs={{4,0},{8,4},{12,8},{5,1},{9,5},{13,9},{6,2},{10,6},{14,10},{7,3},{... | collective-permute-start | bytes 24584 | tf_op jit(solution)/shard_map/ppermute | solution.py:24
  19.0 144.8 %copy-start = (bf16[512,512]{1,0:T(8,128)(2,1)S(1)}, bf16[512,512]{1,0:T(8,128)(2,1)}, u32[]{:S(2)}) copy-start(bf16[512,512]{1,0:T(8,128)(2,1)} %param.19) | copy-start | bytes 1572868
  19.0 199.8 %reduce-scatter.2.cloned.1.call-start = ((), (), s32[]{:S(2)}) async-start(), calls=%async_computation.3 | async-start | bytes 819200 | tf_op jit(solution)/shard_map/reduce_scatter | solution.py:166
  96.0 66.0 %collective-permute-start.3 = (bf16[512,512]{1,0:T(8,128)(2,1)S(1)}, bf16[512,512]{1,0:T(8,128)(2,1)S(1)}, u32[]{:S(2)}, u32[]{:S(2)}) collective-permute-start(bf16[512,512]{1,0:T(8,128)(2,1)S(1)} %collective-permute-done.2), channel_id=1, source_target_pairs={{0,4},{4,8},{8,12},{12,0},{1,5},{5,9},{9,13},{13,1},{2,6},{6,10},{... | collective-permute-start | bytes 1572872 | tf_op jit(solution)/shard_map/ppermute | solution.py:60
  171.4 16.3 %copy-start.5 = (f32[4]{0:T(128)S(1)}, f32[4]{0:T(128)}, u32[]{:S(2)}) copy-start(f32[4]{0:T(128)} %param.16) | copy-start | bytes 52
  171.4 16.6 %copy-start.4 = (f32[4,128]{1,0:T(4,128)S(1)}, f32[4,128]{1,0:T(4,128)}, u32[]{:S(2)}) copy-start(f32[4,128]{1,0:T(4,128)} %param.17) | copy-start | bytes 6148
  187.4 3.0 %copy-start.1 = (bf16[160,512]{1,0:T(8,128)(2,1)S(1)}, bf16[160,512]{1,0:T(8,128)(2,1)}, u32[]{:S(2)}) copy-start(bf16[160,512]{1,0:T(8,128)(2,1)} %constant_dynamic-slice_fusion.1) | copy-start | bytes 491524
  187.4 3.0 %copy-start.2 = (bf16[176,512]{1,0:T(8,128)(2,1)S(1)}, bf16[176,512]{1,0:T(8,128)(2,1)}, u32[]{:S(2)}) copy-start(bf16[176,512]{1,0:T(8,128)(2,1)} %pad_maximum_fusion) | copy-start | bytes 540676
Sparse Core Ops, SparseCore 0:
  9.5 69.5 all-gather.2
  80.7 59.4 all-gather.4
  194.9 23.8 reduce-scatter.1
